TPU v7x, 512 devices: a whole 4x8x8 slice. The times are simulated.
512 devices in a mesh: kv: 64 (over z, y), tp: 8 (over x, core).
Axes of the slice: x: 4, y: 8, z: 8, core: 2. Of those that a mesh axis runs over, the one named last changes fastest.
Arguments:
- tokens: bfloat16 [256, 2048], P('tp', 'kv'), may hold values from -60 to 60
- gain_mix: float32 [2048], P('kv'), may hold values from 0.1 to 1.9
- w_query: bfloat16 [2048, 2048], P('kv', 'tp'), may hold values from -0.125 to 0.125
- w_key: bfloat16 [2048, 2048], P('kv', 'tp'), may hold values from -0.125 to 0.125
- w_value: bfloat16 [2048, 2048], P('kv', 'tp'), may hold values from -0.125 to 0.125
- w_igate: bfloat16 [2048, 8], P('kv', 'tp'), may hold values from -0.125 to 0.125
- w_fgate: bfloat16 [2048, 8], P('kv', 'tp'), may hold values from -0.125 to 0.125
- bias_igate: float32 [8], P('tp'), may hold values from -3 to 3
- bias_fgate: float32 [8], P('tp'), may hold values from -3 to 3
- state_mem: float32 [256, 8, 256, 256], P('kv', 'tp'), may hold values from -2 to 2
- state_max: float32 [256, 8], P('kv', 'tp'), may hold values from -60 to 220
- keys_blk: bfloat16 [256, 8, 128, 256], P('kv', 'tp'), may hold values from -6 to 6
- values_blk: bfloat16 [256, 8, 128, 256], P('kv', 'tp'), may hold values from -6 to 6
- igate_blk: float32 [256, 8, 128], P('kv', 'tp'), may hold values from -10 to 220
- fgate_blk: float32 [256, 8, 128], P('kv', 'tp'), may hold values from -3 to 0
- lengths: int32 [256], P('kv'), may hold values from 1 to 127, 8192 in all
- gain_head: float32 [256], replicated, may hold values from 0.1 to 1.9
- w_mixout: bfloat16 [2048, 2048], P('tp', 'kv'), may hold values from -0.25 to 0.25
- gain_mlp: float32 [2048], P('kv'), may hold values from 0.1 to 1.9
- w_up: bfloat16 [2048, 8192], P('kv', 'tp'), may hold values from -0.125 to 0.125
- w_down: bfloat16 [8192, 2048], P('tp', 'kv'), may hold values from -0.0625 to 0.0625
Outputs:
- layer_out: bfloat16 [256, 2048], P('tp', 'kv')
Inputs may be any that keep to these rules, and one draw needn't show every extreme that they name: `lengths`: entries of a sequence's block at or past its length are not live. The largest length is reached in every draw.
All inputs are finite; a program needn't handle non-finite values.
Results may differ from a plain program's by a relative error of at most 0.015.
Values may be sent and summed in bfloat16 or wider, within the bound.
A program may use at most 64 MiB of HBM per device.

v0:
```python
import jax
import jax.numpy as jnp
from jax import lax
from jax.sharding import PartitionSpec as P

D = 2048


EPS = 1e-06


def sent_to_all(array, axis):
    devices = lax.axis_size(axis)
    return lax.all_to_all(
        jnp.broadcast_to(array[None], (devices, *array.shape)), axis, 0, 0, tiled=True
    )


def joined_along(blocks, dim):
    shape = list(blocks.shape[1:])
    shape[dim] *= blocks.shape[0]
    return jnp.moveaxis(blocks, 0, dim).reshape(shape)


def gather_directly(array, axis, dim):
    blocks = sent_to_all(array, axis)
    return joined_along(blocks, dim)


def split_up(array, dim, devices):
    shape = array.shape
    blocks = array.reshape(*shape[:dim], devices, shape[dim] // devices, *shape[dim + 1 :])
    return jnp.moveaxis(blocks, dim, 0)


def summed_on_arrival(array, axis, dim):
    blocks = split_up(array, dim, lax.axis_size(axis))
    arrived = lax.all_to_all(blocks, axis, split_axis=0, concat_axis=0, tiled=True)
    return arrived.astype(jnp.float32).sum(axis=0)


def sent_together(arrays, axis, dim, along):
    columns = [a.reshape(*a.shape[:along], -1) for a in arrays]
    both = jnp.concatenate(columns, axis=along)
    result, at, finished = (summed_on_arrival(both, axis, dim), 0, [])
    for a, column in zip(arrays, columns):
        slab = result[..., at : at + column.shape[along]]
        finished.append(slab.reshape(*slab.shape[:along], *a.shape[along:]))
        at += column.shape[along]
    return tuple(finished)


def over_copies(array, axis):
    everything = sent_to_all(array, axis)
    return jnp.sum(everything.astype(jnp.float32), axis=0)


def memory_cell(
    query,
    key_new,
    value_new,
    input_gate,
    forget_gate,
    state_mem,
    state_max,
    keys_blk,
    values_blk,
    igate_blk,
    fgate_blk,
    lengths,
    gain_head,
):
    span = keys_blk.shape[2]
    head_size = query.shape[-1]
    positions = jnp.arange(span, dtype=jnp.int32)
    live_mask = positions[None, None, :] < lengths[:, None, None]
    forget_live = jnp.where(live_mask, fgate_blk, 0.0)
    cumulative = jnp.cumsum(forget_live, axis=-1)
    total = cumulative[..., -1]
    suffix = total[..., None] - cumulative + forget_gate[..., None]
    past = igate_blk + suffix
    carried = state_max + total + forget_gate
    topmost = jnp.maximum(
        jnp.maximum(carried, input_gate), jnp.max(jnp.where(live_mask, past, -jnp.inf), axis=-1)
    )
    scale = head_size ** (-0.5)
    scores = (
        jnp.einsum("shd,shbd->shb", query, keys_blk, preferred_element_type=jnp.float32) * scale
    )
    weights = (jnp.where(live_mask, jnp.exp(past - topmost[..., None]), 0.0) * scores).astype(
        jnp.bfloat16
    )
    block_term = jnp.einsum(
        "shb,shbd->shd", weights, values_blk, preferred_element_type=jnp.float32
    )
    query_f = query.astype(jnp.float32)
    state_term = (
        jnp.einsum("shvk,shk->shv", state_mem, query_f, precision=lax.Precision.HIGHEST)
        * jnp.exp(carried - topmost)[..., None]
    )
    own_score = jnp.sum(query_f * key_new.astype(jnp.float32), axis=-1) * scale
    own_term = (jnp.exp(input_gate - topmost) * own_score)[..., None] * value_new.astype(
        jnp.float32
    )
    numerator = state_term + block_term + own_term
    normed = (
        numerator
        * lax.rsqrt(jnp.mean(numerator * numerator, axis=-1, keepdims=True) + EPS)
        * gain_head
    )
    return normed.astype(jnp.bfloat16).reshape(query.shape[0], -1)


def body(
    tokens,
    gain_mix,
    w_query,
    w_key,
    w_value,
    w_igate,
    w_fgate,
    bias_igate,
    bias_fgate,
    state_mem,
    state_max,
    keys_blk,
    values_blk,
    igate_blk,
    fgate_blk,
    lengths,
    gain_head,
    w_mixout,
    gain_mlp,
    w_up,
    w_down,
):
    sequences = state_mem.shape[0]
    head_count = state_mem.shape[1]
    head_size = state_mem.shape[3]
    inner_width = head_count * head_size
    gathered = gather_directly(tokens, "tp", 0)
    widened = gathered.astype(jnp.float32)
    square_in = jnp.sum(widened * widened, axis=1)
    scaled_in = (widened * gain_mix).astype(jnp.bfloat16)
    w_main = jnp.concatenate([w_query, w_key, w_value], axis=1)
    w_gates = jnp.concatenate([w_igate, w_fgate], axis=1)
    main_part = jnp.dot(scaled_in, w_main, preferred_element_type=jnp.float32)
    gate_part = jnp.dot(scaled_in, w_gates, preferred_element_type=jnp.float32)
    main_sum, gate_sum, square_mine = sent_together(
        (
            main_part.astype(jnp.bfloat16),
            gate_part.astype(jnp.bfloat16),
            square_in.astype(jnp.bfloat16),
        ),
        "kv",
        0,
        1,
    )
    factor_in = lax.rsqrt(square_mine / D + EPS)[:, None]
    projected = main_sum * factor_in
    query = (
        projected[:, :inner_width].astype(jnp.bfloat16).reshape(sequences, head_count, head_size)
    )
    key_new = (
        projected[:, inner_width : 2 * inner_width]
        .astype(jnp.bfloat16)
        .reshape(sequences, head_count, head_size)
    )
    value_new = (
        projected[:, 2 * inner_width :]
        .astype(jnp.bfloat16)
        .reshape(sequences, head_count, head_size)
    )
    gate_scaled = gate_sum * factor_in
    input_gate = gate_scaled[:, :head_count] + bias_igate
    forget_gate = jax.nn.log_sigmoid(gate_scaled[:, head_count:] + bias_fgate)
    mixed = memory_cell(
        query,
        key_new,
        value_new,
        input_gate,
        forget_gate,
        state_mem,
        state_max,
        keys_blk,
        values_blk,
        igate_blk,
        fgate_blk,
        lengths,
        gain_head,
    )
    partial_value = jnp.dot(
        gather_directly(mixed, "kv", 0), w_mixout, preferred_element_type=jnp.float32
    )
    attended = over_copies(partial_value.astype(jnp.bfloat16), "tp").astype(jnp.float32)
    residual = (widened + attended).astype(jnp.bfloat16)
    restored = residual.astype(jnp.float32)
    square_mid = jnp.sum(restored * restored, axis=1)
    scaled_mid = (restored * gain_mlp).astype(jnp.bfloat16)
    up_part = jnp.dot(scaled_mid, w_up, preferred_element_type=jnp.float32)
    up_sum, square_sum = sent_together(
        (up_part.astype(jnp.bfloat16), square_mid.astype(jnp.bfloat16)), "kv", 0, 1
    )
    hidden = jnp.square(jax.nn.relu(up_sum * lax.rsqrt(square_sum / D + EPS)[:, None])).astype(
        jnp.bfloat16
    )
    down_part = jnp.dot(
        gather_directly(hidden, "kv", 0), w_down, preferred_element_type=jnp.float32
    )
    down_sum = summed_on_arrival(down_part.astype(jnp.bfloat16), "tp", 0)
    row_count = tokens.shape[0]
    own_rows = lax.dynamic_slice_in_dim(restored, lax.axis_index("tp") * row_count, row_count, 0)
    return (own_rows + down_sum).astype(jnp.bfloat16)


def solution(mesh):
    in_specs = (
        P("tp", "kv"),
        P("kv"),
        P("kv", "tp"),
        P("kv", "tp"),
        P("kv", "tp"),
        P("kv", "tp"),
        P("kv", "tp"),
        P("tp"),
        P("tp"),
        P("kv", "tp", None, None),
        P("kv", "tp"),
        P("kv", "tp", None, None),
        P("kv", "tp", None, None),
        P("kv", "tp", None),
        P("kv", "tp", None),
        P("kv"),
        P(),
        P("tp", "kv"),
        P("kv"),
        P("kv", "tp"),
        P("tp", "kv"),
    )
    out_specs = P("tp", "kv")
    return jax.shard_map(body, mesh=mesh, in_specs=in_specs, out_specs=out_specs, check_vma=False)
```

profile of v0, /device:TPU:1, one launch (start us, length us, event | category | flops | bytes accessed | tf_op | source)
XLA Modules:
  0.0 139.9 jit_solution(15034311884774417352)
XLA Ops:
  0.0 0.9 copy.54
  1.0 13.8 %all_to_all.35 = bf16[8,2,512]{2,1,0:T(2,128)(2,1)S(1)} all-to-all(bf16[8,2,512]{2,1,0:T(2,128)(2,1)S(1)} %reshape.258), channel_id=1, replica_groups=mesh['kv'=64,'tp'=8] {'tp'}, dimensions={0} | all-to-all | bytes 32768 | tf_op jit(solution)/shard_map/all_to_all | solution.py:14
  15.1 1.1 convolution_convert_fusion.1
  16.9 1.0 pad_maximum_fusion.1
  18.0 12.7 %all-to-all-start.1 = ((bf16[64,4,771]{2,1,0:T(4,128)(2,1)}), bf16[64,4,771]{2,1,0:T(4,128)(2,1)S(1)}, u32[]{:S(2)}, u32[]{:S(2)}) async-start(bf16[64,4,771]{2,1,0:T(4,128)(2,1)} %pad_maximum_fusion.1), calls=%async_computation.1 | async-start | bytes 917504 | tf_op jit(solution)/shard_map/all_to_all | solution.py:38
  32.2 1.2 reduce_window_sum.11
  33.6 13.1 %all-to-all-done.1 = bf16[64,4,771]{2,1,0:T(4,128)(2,1)S(1)} async-done(((bf16[64,4,771]{2,1,0:T(4,128)(2,1)}), bf16[64,4,771]{2,1,0:T(4,128)(2,1)S(1)}, u32[]{:S(2)}, u32[]{:S(2)}) %all-to-all-start.1) | async-done | bytes 394784 | tf_op jit(solution)/shard_map/all_to_all | solution.py:38
  46.8 0.2 convert_reduce_fusion.1
  47.4 0.2 fusion.44
  48.2 0.6 fusion
  48.8 0.3 exponential_reduce_fusion
  49.1 0.2 fusion.2
  49.6 17.7 %all_to_all.36 = bf16[64,4,256]{2,1,0:T(4,128)(2,1)S(1)} all-to-all(bf16[64,4,256]{2,1,0:T(4,128)(2,1)S(1)} %broadcast_in_dim.19), channel_id=1, replica_groups=mesh['kv'=64,'tp'=8] {'kv'}, dimensions={0} | all-to-all | bytes 262144 | tf_op jit(solution)/shard_map/all_to_all | solution.py:14
  67.6 10.7 %all_to_all.37 = bf16[8,256,32]{1,2,0:T(8,128)(2,1)S(1)} all-to-all(bf16[8,256,32]{1,2,0:T(8,128)(2,1)S(1)} %broadcast_in_dim.20), channel_id=1, replica_groups=mesh['kv'=64,'tp'=8] {'tp'}, dimensions={0} | all-to-all | bytes 262144 | tf_op jit(solution)/shard_map/all_to_all | solution.py:14
  78.4 0.4 convolution_convert_fusion
  79.2 0.3 pad_maximum_fusion
  79.5 21.8 %all_to_all.38 = bf16[64,4,1025]{2,1,0:T(4,128)(2,1)S(1)} all-to-all(bf16[64,4,1025]{2,1,0:T(4,128)(2,1)S(1)} %pad_maximum_fusion), channel_id=1, replica_groups=mesh['kv'=64,'tp'=8] {'kv'}, dimensions={0} | all-to-all | bytes 1049600 | tf_op jit(solution)/shard_map/all_to_all | solution.py:38
  101.3 0.3 convert_reduce_fusion
  101.9 23.9 %all_to_all.39 = bf16[64,4,1024]{2,1,0:T(4,128)(2,1)S(1)} all-to-all(bf16[64,4,1024]{2,1,0:T(4,128)(2,1)S(1)} %broadcast_in_dim.21), channel_id=1, replica_groups=mesh['kv'=64,'tp'=8] {'kv'}, dimensions={0} | all-to-all | bytes 1048576 | tf_op jit(solution)/shard_map/all_to_all | solution.py:14
  125.9 0.3 convolution_convert_fusion.3
  126.3 0.7 reshape.260
  127.0 7.3 %all-to-all-start.6 = ((bf16[8,2,512]{2,1,0:T(2,128)(2,1)}), bf16[8,2,512]{2,1,0:T(2,128)(2,1)S(1)}, u32[]{:S(2)}, u32[]{:S(2)}) async-start(bf16[8,2,512]{2,1,0:T(2,128)(2,1)} %reshape.260), calls=%async_computation.6 | async-start | bytes 32768 | tf_op jit(solution)/shard_map/all_to_all | solution.py:38
  134.3 4.7 %all-to-all-done.6 = bf16[8,2,512]{2,1,0:T(2,128)(2,1)S(1)} async-done(((bf16[8,2,512]{2,1,0:T(2,128)(2,1)}), bf16[8,2,512]{2,1,0:T(2,128)(2,1)S(1)}, u32[]{:S(2)}, u32[]{:S(2)}) %all-to-all-start.6) | async-done | bytes 16416 | tf_op jit(solution)/shard_map/all_to_all | solution.py:38
  139.2 0.7 copy.66
  (76 shorter events, 4.2 us)
Async XLA Ops:
  0.0 48.2 %copy-start = (f32[4,1,256,256]{3,2,1,0:T(8,128)S(1)}, f32[4,1,256,256]{3,2,1,0:T(8,128)}, u32[]{:S(2)}) copy-start(f32[4,1,256,256]{3,2,1,0:T(8,128)} %param.30) | copy-start | bytes 3145732
  0.0 16.4 %copy-start.9 = (f32[32]{0:T(128)S(1)}, f32[32]{0:T(128)}, u32[]{:S(2)}) copy-start(f32[32]{0:T(128)} %param.22) | copy-start | bytes 388
  0.0 16.4 %copy-start.14 = (bf16[32,1]{0,1:T(2,128)(2,1)S(1)}, bf16[32,1]{0,1:T(2,128)(2,1)}, u32[]{:S(2)}) copy-start(bf16[32,1]{0,1:T(2,128)(2,1)} %param.26) | copy-start | bytes 196
  0.0 16.4 %copy-start.13 = (bf16[32,1]{0,1:T(2,128)(2,1)S(1)}, bf16[32,1]{0,1:T(2,128)(2,1)}, u32[]{:S(2)}) copy-start(bf16[32,1]{0,1:T(2,128)(2,1)} %param.27) | copy-start | bytes 196
  16.4 15.0 %copy-start.10 = (f32[4,1]{0,1:T(1,128)S(1)}, f32[4,1]{0,1:T(1,128)}, u32[]{:S(2)}) copy-start(f32[4,1]{0,1:T(1,128)} %param.31) | copy-start | bytes 52
  16.4 15.8 %copy-start.5 = (s32[4]{0:T(128)S(1)}, s32[4]{0:T(128)}, u32[]{:S(2)}) copy-start(s32[4]{0:T(128)} %param.36) | copy-start | bytes 52
  16.4 15.8 %copy-start.6 = (f32[4,1,128]{2,1,0:T(1,128)S(1)}, f32[4,1,128]{2,1,0:T(1,128)}, u32[]{:S(2)}) copy-start(f32[4,1,128]{2,1,0:T(1,128)} %param.35) | copy-start | bytes 6148
  16.9 30.7 %copy-start.7 = (f32[4,1,128]{2,1,0:T(1,128)S(1)}, f32[4,1,128]{2,1,0:T(1,128)}, u32[]{:S(2)}) copy-start(f32[4,1,128]{2,1,0:T(1,128)} %param.34) | copy-start | bytes 6148
  16.9 31.1 %copy-start.1 = (bf16[4,1,128,256]{3,2,1,0:T(8,128)(2,1)S(1)}, bf16[4,1,128,256]{3,2,1,0:T(8,128)(2,1)}, u32[]{:S(2)}) copy-start(bf16[4,1,128,256]{3,2,1,0:T(8,128)(2,1)} %param.32) | copy-start | bytes 786436
  18.0 28.8 %all-to-all-start.1 = ((bf16[64,4,771]{2,1,0:T(4,128)(2,1)}), bf16[64,4,771]{2,1,0:T(4,128)(2,1)S(1)}, u32[]{:S(2)}, u32[]{:S(2)}) async-start(bf16[64,4,771]{2,1,0:T(4,128)(2,1)} %pad_maximum_fusion.1), calls=%async_computation.1 | async-start | bytes 917504 | tf_op jit(solution)/shard_map/all_to_all | solution.py:38
  30.7 18.4 %copy-start.12 = (bf16[4,1,128,256]{3,2,1,0:T(8,128)(2,1)S(1)}, bf16[4,1,128,256]{3,2,1,0:T(8,128)(2,1)}, u32[]{:S(2)}) copy-start(bf16[4,1,128,256]{3,2,1,0:T(8,128)(2,1)} %param.33) | copy-start | bytes 786436
  33.6 15.8 %copy-start.8 = (f32[256]{0:T(256)S(1)}, f32[256]{0:T(256)}, u32[]{:S(2)}) copy-start(f32[256]{0:T(256)} %param.37) | copy-start | bytes 3076
  48.2 19.2 %copy-start.4 = (bf16[256,32]{0,1:T(8,128)(2,1)S(1)}, bf16[256,32]{0,1:T(8,128)(2,1)}, u32[]{:S(2)}) copy-start(bf16[256,32]{0,1:T(8,128)(2,1)} %param.38) | copy-start | bytes 49156
  48.8 29.6 %copy-start.3 = (bf16[32,1024]{1,0:T(8,128)(2,1)S(1)}, bf16[32,1024]{1,0:T(8,128)(2,1)}, u32[]{:S(2)}) copy-start(bf16[32,1024]{1,0:T(8,128)(2,1)} %param.40) | copy-start | bytes 196612
  48.8 29.6 %copy-start.11 = (f32[32]{0:T(128)S(1)}, f32[32]{0:T(128)}, u32[]{:S(2)}) copy-start(f32[32]{0:T(128)} %param.39) | copy-start | bytes 388
  101.9 24.0 %copy-start.2 = (bf16[1024,32]{0,1:T(8,128)(2,1)S(1)}, bf16[1024,32]{0,1:T(8,128)(2,1)}, u32[]{:S(2)}) copy-start(bf16[1024,32]{0,1:T(8,128)(2,1)} %param.41) | copy-start | bytes 196612
  127.0 12.0 %all-to-all-start.6 = ((bf16[8,2,512]{2,1,0:T(2,128)(2,1)}), bf16[8,2,512]{2,1,0:T(2,128)(2,1)S(1)}, u32[]{:S(2)}, u32[]{:S(2)}) async-start(bf16[8,2,512]{2,1,0:T(2,128)(2,1)} %reshape.260), calls=%async_computation.6 | async-start | bytes 32768 | tf_op jit(solution)/shard_map/all_to_all | solution.py:38
where the time goes:
time: 140 us
  blocking collectives  87.9 us (63%)
  starting transfers between devices  20 us (14%)
  waiting for transfers between devices  17.8 us (13%)
  other arithmetic  4.86 us (3%)
  local copies, waits for them, and re-layouts  4.6 us (3%)
  matrix products  3.06 us (2%)
  between operations  1.72 us (1%)
    all_to_all x4, blocking collectives, sent_to_all(): lax.all_to_all(jnp.broadcast_to(array[None], (devices, *array.shape)), ax...  66.1 us
    all_to_all x1, blocking collectives, summed_on_arrival(): lax.all_to_all(blocks, axis, split_axis=0, concat_axis=0, tiled=True)  21.8 us
    all_to_all x2, starting transfers between devices, summed_on_arrival(): lax.all_to_all(blocks, axis, split_axis=0, concat_axis=0, tiled=True)  20 us
    all_to_all x2, waiting for transfers between devices, summed_on_arrival(): lax.all_to_all(blocks, axis, split_axis=0, concat_axis=0, tiled=True)  17.8 us
  transfers between devices with their start and end apart: 2, of which 2 were waited for; matrix products, arithmetic and copies ran while one was open for 1% of the time, Pallas kernels for 0%

commit v1 on v0

v1 whole, which is shorter than its diff:
```python
import jax
import jax.numpy as jnp
from jax import lax
from jax.experimental import pallas as pl
from jax.experimental.pallas import tpu as pltpu
from jax.sharding import PartitionSpec as P

MESH = pl.DeviceIdType.MESH
F32, BF16 = jnp.float32, jnp.bfloat16
D = 2048
EPS = 1e-06
SCALE = 256 ** (-0.5)


def at_lanes(rows, offset, width):
    lane = lax.broadcasted_iota(jnp.int32, (rows, width), 1)
    row = lax.broadcasted_iota(jnp.int32, (rows, width), 0)
    return jnp.where(lane == row + offset, 1.0, 0.0)


def contract_last(a, b):
    return lax.dot_general(a, b, (((1,), (1,)), ((), ())), preferred_element_type=F32)


def column(row_ref, rows):
    n = row_ref.shape[1]
    v = jnp.broadcast_to(row_ref[...].astype(F32), (rows, n))
    lane = lax.broadcasted_iota(jnp.int32, (rows, n), 1)
    row = lax.broadcasted_iota(jnp.int32, (rows, n), 0)
    return jnp.sum(jnp.where(lane == row, v, 0.0), axis=1, keepdims=True)


def kernel(
    tok_h, gmix_h, wq_h, wk_h, wv_h, wi_h, wf_h, bi_h, bf_h, st_h, smax_h, k_h, v_h, ig_h, fg_h, len_h, gh_h, wm_h, gm_h,
    wu_h, wd_h, out_ref,
    tok, gmix, wi, wf, bi, bfg, st, smax, kb, vb, igb, fgb, lens, gh, gm,
    w1g, w2g, wmg, wug, wdg,
    ma, ra, a2, sb, rb, xraw, xsc, mz1, rz1, mz2, rz2, slo, shi, rows8, q16, w16, mc, rc, m32, md, rd, res, mf, rf, mg, rg, h32,
    mh, rh, mi, ri,
    lsem, ssem, rsem,
):
    kv = lax.axis_index("kv")
    t = lax.axis_index("tp")
    z = lax.shift_right_logical(kv, 3)
    y = lax.bitwise_and(kv, 7)
    zs = lambda i: (lax.bitwise_xor(kv, 8 * i), t)
    ys = lambda i: (lax.bitwise_xor(kv, i), t)
    ts = lambda i: (kv, lax.bitwise_xor(t, i))

    barrier = pltpu.get_barrier_semaphore()
    for who in (ys, ts, zs):
        for i in range(1, 8):
            pl.semaphore_signal(barrier, inc=1, device_id=who(i), device_id_type=MESH)

    loads = []

    def load(src, dst):
        c = pltpu.make_async_copy(src, dst, lsem.at[len(loads)])
        c.start()
        loads.append(c)
        return c

    l_tok = load(tok_h, tok)
    l_gmix = load(gmix_h, gmix)
    l_wi = load(wi_h, wi)
    l_wf = load(wf_h, wf)
    l_gm = load(gm_h, gm)
    l_w1 = load(wq_h, w1g.at[y])
    l_wk = load(wk_h, w2g.at[y, :, pl.ds(0, 256)])
    l_wv = load(wv_h, w2g.at[y, :, pl.ds(256, 256)])
    l_wm = load(wm_h, wmg.at[y])
    l_wu = load(wu_h, wug.at[y])
    l_wd = load(wd_h, wdg.at[y])
    cell = [
        load(a, b)
        for a, b in (
            (st_h, st), (smax_h, smax), (k_h, kb), (v_h, vb), (ig_h, igb), (fg_h, fgb), (len_h, lens), (gh_h, gh),
            (bi_h, bi), (bf_h, bfg),
        )
    ]

    pending = []

    def send(n, src, dst, who):
        for i in range(1, 8):
            c = pltpu.make_async_remote_copy(
                src_ref=src(i), dst_ref=dst, send_sem=ssem.at[n], recv_sem=rsem.at[n], device_id=who(i), device_id_type=MESH
            )
            c.start()
        pending.append((n, dst))

    def arrive(n, buf):
        part = buf.at[pl.ds(0, 7)]
        pltpu.make_async_copy(part, part, rsem.at[n]).wait()

    def left(n, buf):
        part = buf.at[pl.ds(0, 7)]
        pltpu.make_async_copy(part, part, ssem.at[n]).wait()

    place = at_lanes(32, 32 * y, 256)
    place_b = place.astype(BF16)
    l_tok.wait()
    l_gmix.wait()
    raw = tok[...].astype(F32)
    scaled = (raw * gmix[...]).astype(BF16)
    raw_p = jnp.dot(tok[...], place_b, preferred_element_type=F32)
    sc_p = jnp.dot(scaled, place_b, preferred_element_type=F32)
    for j in range(8):
        both = jnp.concatenate([raw_p[4 * j : 4 * j + 4], sc_p[4 * j : 4 * j + 4]], axis=0)
        ma[j] = both.astype(BF16)
    ra[y] = ma[y]

    l_wi.wait()
    l_wf.wait()
    l_gm.wait()
    g0 = gm[...]
    g1 = g0.astype(BF16).astype(F32)
    g2 = (g0 - g1).astype(BF16).astype(F32)
    g3 = g0 - g1 - g2
    row8 = lax.broadcasted_iota(jnp.int32, (8, 32), 0)
    six = jnp.zeros((8, 32), F32)
    for r, v in enumerate((wi[...].astype(F32), wf[...].astype(F32), g1, g2, g3)):
        six = jnp.where(row8 == r, jnp.broadcast_to(v, (8, 32)), six)
    a2[y] = jnp.dot(six.astype(BF16), place_b, preferred_element_type=F32).astype(BF16)

    l_w1.wait()
    l_wk.wait()
    l_wv.wait()
    pl.semaphore_wait(barrier, 21)

    send(0, lambda i: ma.at[lax.bitwise_xor(y, i)], ra.at[y], ys)
    send(1, lambda i: a2.at[y], a2.at[y], ys)
    send(2, lambda i: w1g.at[y], w1g.at[y], ys)
    send(3, lambda i: w2g.at[y], w2g.at[y], ys)

    for c in cell:
        c.wait()
    for s in range(4):
        hi = st[s, 0].astype(BF16)
        shi[s] = hi
        slo[s] = (st[s, 0] - hi.astype(F32)).astype(BF16)
    rows8[...] = jnp.zeros(rows8.shape, F32)
    for s in range(4):
        rows8[0, s : s + 1, :] = igb[s]
        rows8[1, s : s + 1, :] = fgb[s]
    lane = lax.broadcasted_iota(jnp.int32, (8, 128), 1)
    row = lax.broadcasted_iota(jnp.int32, (8, 128), 0)
    live = lane.astype(F32) < column(lens, 8)
    forget_live = jnp.where(live, rows8[1], 0.0)
    total = jnp.sum(forget_live, axis=1, keepdims=True)
    after = jnp.where(
        lax.broadcasted_iota(jnp.int32, (128, 128), 0) > lax.broadcasted_iota(jnp.int32, (128, 128), 1), 1.0, 0.0
    )
    past0 = rows8[0] + jnp.dot(forget_live, after, precision=lax.Precision.HIGHEST, preferred_element_type=F32)
    past0_top = jnp.max(jnp.where(live, past0, -1e30), axis=1, keepdims=True)
    carried0 = column(smax, 8) + total
    q16[...] = jnp.zeros(q16.shape, F32)
    w16[...] = jnp.zeros(w16.shape, F32)

    arrive(0, ra)
    joined = ra[0].astype(F32)
    for j in range(1, 8):
        joined += ra[j].astype(F32)
    sb[...] = joined.astype(BF16)
    rb[t] = joined.astype(BF16)
    send(4, lambda i: sb, rb.at[t], ts)
    l_wm.wait()
    send(5, lambda i: wmg.at[y], wmg.at[y], ys)

    arrive(4, rb)
    squares = []
    for j in range(8):
        b = rb[j].astype(F32)
        xraw[4 * j : 4 * j + 4, :] = b[0:4]
        xsc[4 * j : 4 * j + 4, :] = b[4:8]
    square_in = jnp.sum(xraw[...] * xraw[...], axis=1, keepdims=True)
    x = xsc[...].astype(BF16)
    arrive(1, a2)
    small = a2[0].astype(F32)
    for j in range(1, 8):
        small += a2[j].astype(F32)
    wgates = jnp.concatenate([small, jnp.zeros((120, 256), F32)], axis=0).astype(BF16)
    gain_mid = small[2:3] + small[3:4] + small[4:5]
    lane32 = lax.broadcasted_iota(jnp.int32, (32, 128), 1)

    def with_square(block, sq, at):
        hi = sq.astype(BF16).astype(F32)
        return jnp.where(lane32 == at, hi, jnp.where(lane32 == at + 1, sq - hi, block))

    gates = with_square(contract_last(x, wgates), square_in, 2)
    arrive(2, w1g)
    q_part = jnp.dot(x, w1g[...].reshape(256, 256), preferred_element_type=F32)
    for j in range(8):
        mz1[j, :, 0:256] = q_part[4 * j : 4 * j + 4].astype(BF16)
        mz1[j, :, 256:384] = gates[4 * j : 4 * j + 4].astype(BF16)
    rz1[z] = mz1[z]
    send(6, lambda i: mz1.at[lax.bitwise_xor(z, i)], rz1.at[z], zs)
    l_wu.wait()
    send(7, lambda i: wug.at[y], wug.at[y], ys)
    arrive(3, w2g)
    kv_part = jnp.dot(x, w2g[...].reshape(256, 512), preferred_element_type=F32)
    for j in range(8):
        mz2[j] = kv_part[4 * j : 4 * j + 4].astype(BF16)
    rz2[z] = mz2[z]
    send(8, lambda i: mz2.at[lax.bitwise_xor(z, i)], rz2.at[z], zs)
    l_wd.wait()
    send(9, lambda i: wdg.at[y], wdg.at[y], ys)

    arrive(6, rz1)
    first = rz1[0].astype(F32)
    for j in range(1, 8):
        first += rz1[j].astype(F32)
    own = first[:, 256:384]
    factor = lax.rsqrt((own[:, 2:3] + own[:, 3:4]) / D + EPS)
    q16[0:4, :] = first[:, 0:256] * factor
    rows8[2, 0:4, :] = own * factor
    gate8 = rows8[2]
    input_gate = gate8[:, 0:1] + bi[...]
    pre = gate8[:, 1:2] + bfg[...]
    forget_gate = jnp.minimum(pre, 0.0) - jnp.log1p(jnp.exp(-jnp.abs(pre)))
    carried = carried0 + forget_gate
    topmost = jnp.maximum(jnp.maximum(carried, input_gate), past0_top + forget_gate)
    decay = jnp.where(live, jnp.exp(jnp.minimum(past0 + forget_gate - topmost, 0.0)), 0.0)
    qb = q16[...].astype(BF16)
    scores = jnp.zeros((8, 128), F32)
    state = jnp.zeros((8, 256), F32)
    row256 = lax.broadcasted_iota(jnp.int32, (8, 256), 0)
    for s in range(4):
        scores = jnp.where(row == s, contract_last(qb, kb[s, 0])[0:8], scores)
        part = contract_last(qb, shi[s])[0:8] + contract_last(qb, slo[s])[0:8]
        state = jnp.where(row256 == s, part, state)
    w16[0:8, :] = decay * (scores * SCALE)
    wb = w16[...].astype(BF16)
    block = jnp.zeros((8, 256), F32)
    for s in range(4):
        block = jnp.where(row256 == s, jnp.dot(wb, vb[s, 0], preferred_element_type=F32)[0:8], block)
    numerator = jnp.exp(carried - topmost) * state + block
    own_scale = jnp.exp(input_gate - topmost) * SCALE

    arrive(8, rz2)
    second = rz2[0].astype(F32)
    for j in range(1, 8):
        second += rz2[j].astype(F32)
    second = (second * factor).astype(BF16).astype(F32)
    own_score = jnp.sum(qb[0:4].astype(F32) * second[:, 0:256], axis=1, keepdims=True)
    num = numerator[0:4] + (own_scale[0:4] * own_score) * second[:, 256:512]
    mixed = num * lax.rsqrt(jnp.mean(num * num, axis=1, keepdims=True) + EPS) * gh[...]
    mc[...] = mixed.astype(BF16)
    rc[z] = mixed.astype(BF16)
    send(10, lambda i: mc, rc.at[z], zs)

    arrive(5, wmg)
    arrive(10, rc)
    for j in range(8):
        m32[4 * j : 4 * j + 4, :] = rc[j].astype(F32)
    att = contract_last(m32[...].astype(BF16), wmg[...].reshape(256, 256)).astype(BF16)
    md[...] = att
    rd[t] = att
    send(11, lambda i: md, rd.at[t], ts)
    arrive(11, rd)
    attended = rd[0].astype(F32)
    for j in range(1, 8):
        attended += rd[j].astype(F32)
    restored = (xraw[...] + attended).astype(BF16).astype(F32)
    for j in range(8):
        res[j] = restored[4 * j : 4 * j + 4]

    square_mid = jnp.sum(restored * restored, axis=1, keepdims=True)
    sq_block = with_square(jnp.zeros((32, 128), F32), square_mid, 0)
    arrive(7, wug)
    up = jnp.dot((restored * gain_mid).astype(BF16), wug[...].reshape(256, 1024), preferred_element_type=F32)
    for j in range(8):
        mf[j, :, 0:1024] = up[4 * j : 4 * j + 4].astype(BF16)
        mf[j, :, 1024:1152] = sq_block[4 * j : 4 * j + 4].astype(BF16)
    rf[z] = mf[z]
    send(12, lambda i: mf.at[lax.bitwise_xor(z, i)], rf.at[z], zs)
    arrive(12, rf)
    whole = rf[0].astype(F32)
    for j in range(1, 8):
        whole += rf[j].astype(F32)
    factor_mid = lax.rsqrt((whole[:, 1024:1025] + whole[:, 1025:1026]) / D + EPS)
    hid = jnp.square(jnp.maximum(whole[:, 0:1024] * factor_mid, 0.0)).astype(BF16)
    mg[...] = hid
    rg[z] = hid
    send(13, lambda i: mg, rg.at[z], zs)

    arrive(9, wdg)
    arrive(13, rg)
    for j in range(8):
        h32[4 * j : 4 * j + 4, :] = rg[j].astype(F32)
    down = contract_last(h32[...].astype(BF16), wdg[...].reshape(256, 1024))
    for j in range(8):
        mh[j] = down[4 * j : 4 * j + 4].astype(BF16)
    rh[t] = mh[t]
    send(14, lambda i: mh.at[lax.bitwise_xor(t, i)], rh.at[t], ts)
    arrive(14, rh)
    last = res[t]
    summed = rh[0].astype(F32)
    for j in range(1, 8):
        summed += rh[j].astype(F32)
    done = (last + summed).astype(BF16)
    mi[...] = done
    ri[y] = done
    send(15, lambda i: mi, ri.at[y], ys)
    arrive(15, ri)
    for j in range(8):
        m32[4 * j : 4 * j + 4, :] = ri[j].astype(F32)
    out_ref[...] = contract_last(m32[...].astype(BF16), place_b)

    for n, buf in (
        (0, ra), (1, a2), (2, w1g), (3, w2g), (4, rb), (5, wmg), (6, rz1), (7, wug), (8, rz2), (9, wdg), (10, rc), (11, rd),
        (12, rf), (13, rg), (14, rh), (15, ri),
    ):
        left(n, buf)


def body(
    tokens, gain_mix, w_query, w_key, w_value, w_igate, w_fgate, bias_igate, bias_fgate, state_mem, state_max, keys_blk,
    values_blk, igate_blk, fgate_blk, lengths, gain_head, w_mixout, gain_mlp, w_up, w_down,
):
    args = (
        tokens, gain_mix.reshape(1, 32), w_query, w_key, w_value, w_igate.T, w_fgate.T, bias_igate.reshape(1, 1),
        bias_fgate.reshape(1, 1), state_mem, state_max.T, keys_blk, values_blk, igate_blk, fgate_blk, lengths.reshape(1, 4),
        gain_head.reshape(1, 256), w_mixout.T, gain_mlp.reshape(1, 32), w_up, w_down.T,
    )
    vm = pltpu.VMEM
    out = pl.pallas_call(
        kernel,
        out_shape=jax.ShapeDtypeStruct((32, 32), F32),
        in_specs=[pl.BlockSpec(memory_space=pl.ANY)] * 21,
        out_specs=pl.BlockSpec(memory_space=pltpu.VMEM),
        scratch_shapes=[
            vm((32, 32), BF16), vm((1, 32), F32), vm((1, 32), BF16), vm((1, 32), BF16), vm((1, 1), F32), vm((1, 1), F32),
            vm((4, 1, 256, 256), F32), vm((1, 4), F32), vm((4, 1, 128, 256), BF16), vm((4, 1, 128, 256), BF16),
            vm((4, 1, 128), F32), vm((4, 1, 128), F32), vm((1, 4), jnp.int32), vm((1, 256), F32), vm((1, 32), F32),
            vm((8, 32, 256), BF16), vm((8, 32, 512), BF16), vm((8, 32, 256), BF16), vm((8, 32, 1024), BF16),
            vm((8, 32, 1024), BF16),
            vm((8, 8, 256), BF16), vm((8, 8, 256), BF16), vm((8, 8, 256), BF16), vm((8, 256), BF16), vm((8, 8, 256), BF16),
            vm((32, 256), F32), vm((32, 256), F32), vm((8, 4, 384), BF16), vm((8, 4, 384), BF16), vm((8, 4, 512), BF16),
            vm((8, 4, 512), BF16), vm((4, 256, 256), BF16), vm((4, 256, 256), BF16), vm((3, 8, 128), F32), vm((16, 256), F32),
            vm((16, 128), F32), vm((4, 256), BF16), vm((8, 4, 256), BF16), vm((32, 256), F32), vm((32, 256), BF16),
            vm((8, 32, 256), BF16), vm((8, 4, 256), F32), vm((8, 4, 1152), BF16), vm((8, 4, 1152), BF16), vm((4, 1024), BF16),
            vm((8, 4, 1024), BF16), vm((32, 1024), F32), vm((8, 4, 256), BF16), vm((8, 4, 256), BF16), vm((4, 256), BF16),
            vm((8, 4, 256), BF16),
            pltpu.SemaphoreType.DMA((21,)), pltpu.SemaphoreType.DMA((16,)), pltpu.SemaphoreType.DMA((16,)),
        ],
        compiler_params=pltpu.CompilerParams(collective_id=0, has_side_effects=True),
    )(*args)
    return out.astype(BF16)


def solution(mesh):
    in_specs = (
        P("tp", "kv"),
        P("kv"),
        P("kv", "tp"),
        P("kv", "tp"),
        P("kv", "tp"),
        P("kv", "tp"),
        P("kv", "tp"),
        P("tp"),
        P("tp"),
        P("kv", "tp", None, None),
        P("kv", "tp"),
        P("kv", "tp", None, None),
        P("kv", "tp", None, None),
        P("kv", "tp", None),
        P("kv", "tp", None),
        P("kv"),
        P(),
        P("tp", "kv"),
        P("kv"),
        P("kv", "tp"),
        P("tp", "kv"),
    )
    return jax.shard_map(body, mesh=mesh, in_specs=in_specs, out_specs=P("tp", "kv"), check_vma=False)
```

time: 140 us -> 68.6 us (0.49)
  blocking collectives: 87.9 us -> 0 us
  Pallas kernels: 0 us -> 65.7 us
  starting transfers between devices: 20 us -> 0 us
  waiting for transfers between devices: 17.8 us -> 0 us
  local copies, waits for them, and re-layouts: 4.6 us -> 0 us
  other arithmetic: 4.86 us -> 1.32 us
  matrix products: 3.06 us -> 0 us
    all_to_all x5 -> x0, blocking collectives: 87.9 us -> none  [the longest x4 66.1 us: sent_to_all(): lax.all_to_all(jnp.broadcast_to(array[None], (devices, *array.shape)), ax...]
    pallas_call x0 -> x1, Pallas kernels: none -> 65.7 us  [body(): pl.pallas_call(kernel, out_shape=jax.ShapeDtypeStruct((32, 32), F32), in_...]
    all_to_all x2 -> x0, starting transfers between devices: 20 us -> none  [summed_on_arrival(): lax.all_to_all(blocks, axis, split_axis=0, concat_axis=0, tiled=True)]
    all_to_all x2 -> x0, waiting for transfers between devices: 17.8 us -> none  [summed_on_arrival(): lax.all_to_all(blocks, axis, split_axis=0, concat_axis=0, tiled=True)]
    dot_general x8 -> x0, matrix products: 3.06 us -> none  [the longest x1 1.12 us: body(): main_part = jnp.dot(scaled_in, w_main, preferred_element_type=jnp.float32)]
    unnamed x37 -> x0, local copies, waits for them, and re-layouts: 2.07 us -> none
  transfers between devices with their start and end apart: 2 -> 0, of which waited for: 2 -> 0; matrix products, arithmetic and copies ran while one was open for 1% -> 0% of each run, Pallas kernels for 0% -> 0%
where the time goes in v1:
time: 68.6 us; the launch traced here: 68.4 us
  Pallas kernels  65.7 us (96%)
  other arithmetic  1.32 us (2%)
  between operations  1.3 us (2%)
    pallas_call x1, Pallas kernels, body(): pl.pallas_call(kernel, out_shape=jax.ShapeDtypeStruct((32, 32), F32), in_...  65.7 us

profile of v1, /device:TPU:1, one launch (start us, length us, event | category | flops | bytes accessed | tf_op | source)
XLA Modules:
  0.0 68.4 jit_solution(7464565191097496502)
XLA Ops:
  1.3 65.7 %shard_map.199 = f32[32,32]{1,0:T(8,128)} custom-call(bf16[32,32]{1,0:T(8,128)(2,1)} %tok_h.1, f32[1,32]{1,0:T(1,128)} %bitcast.16, bf16[32,256]{1,0:T(8,128)(2,1)} %wq_h.1, bf16[32,256]{1,0:T(8,128)(2,1)} %wk_h.1, bf16[32,256]{1,0:T(8,128)(2,1)} %wv_h.1, bf16[1,32]{1,0:T(2,128)(2,1)} %bitcast.17, bf16[1,32]{1,0:T(2,128)(2,1)} %bitcast.18, ...), custom_call_target="tpu_custom_call" | custom-call | tf_op jit(solution)/shard_map/pallas_call | solution.py:327
  67.0 1.3 %convert_element_type.3 = bf16[32,32]{1,0:T(8,128)(2,1)} convert(f32[32,32]{1,0:T(8,128)} %shard_map.199) | non-fusion elementwise | flops 1024 | bytes 6144 | tf_op jit(solution)/shard_map/convert_element_type | solution.py:349

commit v2 on v1

--- a/solution.py
+++ b/solution.py
@@ -35,8 +35,8 @@
     wu_h, wd_h, out_ref,
     tok, gmix, wi, wf, bi, bfg, st, smax, kb, vb, igb, fgb, lens, gh, gm,
     w1g, w2g, wmg, wug, wdg,
-    ma, ra, a2, sb, rb, xraw, xsc, mz1, rz1, mz2, rz2, slo, shi, rows8, q16, w16, mc, rc, m32, md, rd, res, mf, rf, mg, rg, h32,
-    mh, rh, mi, ri,
+    ma, ra, a2, xraw, mz1, rz1, mz2, rz2, slo, shi, rows8, q16, w16, mc, rc, m32, md, rd, mf, rf, mg, rg, h32,
+    mh, rh, mp, rp,
     lsem, ssem, rsem,
 ):
     kv = lax.axis_index("kv")
@@ -47,10 +47,23 @@
     ys = lambda i: (lax.bitwise_xor(kv, i), t)
     ts = lambda i: (kv, lax.bitwise_xor(t, i))
 
+    far = z != t
+    rows_to = lambda i: (8 * t + y, lax.bitwise_xor(t, i))
+    rows_of = lambda i: (lax.bitwise_xor(kv, 8 * i), z)
+
     barrier = pltpu.get_barrier_semaphore()
-    for who in (ys, ts, zs):
+
+    def greet(who):
+        pl.semaphore_signal(barrier, inc=1, device_id=who, device_id_type=MESH)
+
+    for who in (rows_to, rows_of, ys, zs, ts):
         for i in range(1, 8):
-            pl.semaphore_signal(barrier, inc=1, device_id=who(i), device_id_type=MESH)
+            greet(who(i))
+
+    @pl.when(far)
+    def _():
+        greet(rows_to(0))
+        greet(rows_of(0))
 
     loads = []
 
@@ -65,12 +78,12 @@
     l_wi = load(wi_h, wi)
     l_wf = load(wf_h, wf)
     l_gm = load(gm_h, gm)
-    l_w1 = load(wq_h, w1g.at[y])
-    l_wk = load(wk_h, w2g.at[y, :, pl.ds(0, 256)])
-    l_wv = load(wv_h, w2g.at[y, :, pl.ds(256, 256)])
-    l_wm = load(wm_h, wmg.at[y])
-    l_wu = load(wu_h, wug.at[y])
-    l_wd = load(wd_h, wdg.at[y])
+    l_w1 = load(wq_h, w1g.at[z])
+    l_wk = load(wk_h, w2g.at[z, :, pl.ds(0, 256)])
+    l_wv = load(wv_h, w2g.at[z, :, pl.ds(256, 256)])
+    l_wm = load(wm_h, wmg.at[z])
+    l_wu = load(wu_h, wug.at[z])
+    l_wd = load(wd_h, wdg.at[z])
     cell = [
         load(a, b)
         for a, b in (
@@ -79,17 +92,19 @@
         )
     ]
 
-    pending = []
-
-    def send(n, src, dst, who):
+    pending, arrived = [], set()
+
+    def send(n, src, buf, slot, who):
+        dst = buf.at[slot]
         for i in range(1, 8):
             c = pltpu.make_async_remote_copy(
                 src_ref=src(i), dst_ref=dst, send_sem=ssem.at[n], recv_sem=rsem.at[n], device_id=who(i), device_id_type=MESH
             )
             c.start()
-        pending.append((n, dst))
+        pending.append((n, buf))
 
     def arrive(n, buf):
+        arrived.add(n)
         part = buf.at[pl.ds(0, 7)]
         pltpu.make_async_copy(part, part, rsem.at[n]).wait()
 
@@ -97,41 +112,92 @@
         part = buf.at[pl.ds(0, 7)]
         pltpu.make_async_copy(part, part, ssem.at[n]).wait()
 
-    place = at_lanes(32, 32 * y, 256)
-    place_b = place.astype(BF16)
+    def start_one(n, src, dst, who):
+        pltpu.make_async_remote_copy(
+            src_ref=src, dst_ref=dst, send_sem=ssem.at[n], recv_sem=rsem.at[n], device_id=who, device_id_type=MESH
+        ).start()
+
+    def send_cross(n, src, buf, slot, who):
+        for i in range(1, 8):
+            start_one(n, src(i), buf.at[slot], who(i))
+
+        @pl.when(far)
+        def _():
+            start_one(n, src(0), buf.at[slot], who(0))
+
+        @pl.when(z == t)
+        def _():
+            buf[slot] = src(0)[...]
+
+    zn = lambda k: lax.bitwise_and(z + k, 7)
+    on_z = lambda k: (8 * zn(k) + y, t)
+
+    def relay_copy(n, chunk, who, sem):
+        pltpu.make_async_remote_copy(
+            src_ref=chunk, dst_ref=chunk, send_sem=ssem.at[n], recv_sem=rsem.at[sem], device_id=who, device_id_type=MESH
+        ).start()
+
+    def spread(n, buf):
+        for k in (2, -2, 1, -1):
+            relay_copy(n, buf.at[z], on_z(k), n if abs(k) == 2 else 16 + n)
+        pending.append((n, buf))
+        arrived.add(n)
+
+    def relay(n, buf):
+        part = buf.at[pl.ds(0, 2)]
+        pltpu.make_async_copy(part, part, rsem.at[n]).wait()
+        half = buf.shape[2] // 2
+        relay_copy(n, buf.at[zn(-2)], on_z(1), 32 + n)
+        relay_copy(n, buf.at[zn(2)], on_z(-1), 32 + n)
+        relay_copy(n, buf.at[zn(-2), :, pl.ds(0, half)], on_z(2), 32 + n)
+        relay_copy(n, buf.at[zn(2), :, pl.ds(half, half)], on_z(-2), 32 + n)
+
+    def collected(n, buf):
+        part = buf.at[pl.ds(0, 2)]
+        pltpu.make_async_copy(part, part, rsem.at[16 + n]).wait()
+        part = buf.at[pl.ds(0, 3)]
+        pltpu.make_async_copy(part, part, rsem.at[32 + n]).wait()
+
+    def cross_done(sem, buf):
+        @pl.when(far)
+        def _():
+            pltpu.make_async_copy(buf, buf, sem).wait()
+
+        @pl.when(z == t)
+        def _():
+            part = buf.at[pl.ds(0, 7)]
+            pltpu.make_async_copy(part, part, sem).wait()
+
     l_tok.wait()
-    l_gmix.wait()
-    raw = tok[...].astype(F32)
-    scaled = (raw * gmix[...]).astype(BF16)
-    raw_p = jnp.dot(tok[...], place_b, preferred_element_type=F32)
-    sc_p = jnp.dot(scaled, place_b, preferred_element_type=F32)
-    for j in range(8):
-        both = jnp.concatenate([raw_p[4 * j : 4 * j + 4], sc_p[4 * j : 4 * j + 4]], axis=0)
-        ma[j] = both.astype(BF16)
-    ra[y] = ma[y]
+    placed = jnp.dot(
+        tok[...], at_lanes(32, 32 * lax.bitwise_and(z, 1), 128).astype(BF16), preferred_element_type=F32
+    )
+    ma[...] = (placed[0:16] + pltpu.roll(placed[16:32], 64, 1)).astype(BF16)
+    pl.semaphore_wait(barrier, 37 - 2 * (z == t).astype(jnp.int32))
+    send_cross(0, lambda i: ma, ra, z, rows_to)
 
     l_wi.wait()
     l_wf.wait()
     l_gm.wait()
-    g0 = gm[...]
-    g1 = g0.astype(BF16).astype(F32)
-    g2 = (g0 - g1).astype(BF16).astype(F32)
-    g3 = g0 - g1 - g2
+    l_gmix.wait()
+
+    def parts(g):
+        first = g.astype(BF16).astype(F32)
+        second = (g - first).astype(BF16).astype(F32)
+        return first, second, g - first - second
+
+    place = at_lanes(32, 32 * lax.bitwise_and(z, 3), 128).astype(BF16)
     row8 = lax.broadcasted_iota(jnp.int32, (8, 32), 0)
-    six = jnp.zeros((8, 32), F32)
-    for r, v in enumerate((wi[...].astype(F32), wf[...].astype(F32), g1, g2, g3)):
-        six = jnp.where(row8 == r, jnp.broadcast_to(v, (8, 32)), six)
-    a2[y] = jnp.dot(six.astype(BF16), place_b, preferred_element_type=F32).astype(BF16)
-
+    eight = jnp.zeros((8, 32), F32)
+    for r, v in enumerate((wi[...].astype(F32), wf[...].astype(F32), *parts(gm[...]), *parts(gmix[...]))):
+        eight = jnp.where(row8 == r, jnp.broadcast_to(v, (8, 32)), eight)
+    a2[z] = jnp.dot(eight.astype(BF16), place, preferred_element_type=F32).astype(BF16)
+    send(1, lambda i: a2.at[z], a2, z, zs)
     l_w1.wait()
+    spread(2, w1g)
     l_wk.wait()
     l_wv.wait()
-    pl.semaphore_wait(barrier, 21)
-
-    send(0, lambda i: ma.at[lax.bitwise_xor(y, i)], ra.at[y], ys)
-    send(1, lambda i: a2.at[y], a2.at[y], ys)
-    send(2, lambda i: w1g.at[y], w1g.at[y], ys)
-    send(3, lambda i: w2g.at[y], w2g.at[y], ys)
+    spread(3, w2g)
 
     for c in cell:
         c.wait()
@@ -157,30 +223,30 @@
     q16[...] = jnp.zeros(q16.shape, F32)
     w16[...] = jnp.zeros(w16.shape, F32)
 
-    arrive(0, ra)
-    joined = ra[0].astype(F32)
-    for j in range(1, 8):
-        joined += ra[j].astype(F32)
-    sb[...] = joined.astype(BF16)
-    rb[t] = joined.astype(BF16)
-    send(4, lambda i: sb, rb.at[t], ts)
+    relay(2, w1g)
+    relay(3, w2g)
     l_wm.wait()
-    send(5, lambda i: wmg.at[y], wmg.at[y], ys)
-
-    arrive(4, rb)
-    squares = []
-    for j in range(8):
-        b = rb[j].astype(F32)
-        xraw[4 * j : 4 * j + 4, :] = b[0:4]
-        xsc[4 * j : 4 * j + 4, :] = b[4:8]
-    square_in = jnp.sum(xraw[...] * xraw[...], axis=1, keepdims=True)
-    x = xsc[...].astype(BF16)
+    spread(5, wmg)
+    cross_done(rsem.at[0], ra)
+    low = lax.broadcasted_iota(jnp.int32, (16, 128), 1) < 64
+    for h in range(2):
+        one = ra[4 * h].astype(F32) + ra[4 * h + 1].astype(F32)
+        two = ra[4 * h + 2].astype(F32) + ra[4 * h + 3].astype(F32)
+        xraw[0:16, 128 * h : 128 * h + 128] = jnp.where(low, one, pltpu.roll(two, 64, 1))
+        xraw[16:32, 128 * h : 128 * h + 128] = jnp.where(low, pltpu.roll(one, 64, 1), two)
+    xr = xraw[...]
+    square_in = jnp.sum(xr * xr, axis=1, keepdims=True)
     arrive(1, a2)
-    small = a2[0].astype(F32)
-    for j in range(1, 8):
-        small += a2[j].astype(F32)
+    halves = []
+    for h in range(2):
+        half = a2[4 * h].astype(F32)
+        for j in range(1, 4):
+            half += a2[4 * h + j].astype(F32)
+        halves.append(half)
+    small = jnp.concatenate(halves, axis=1)
     wgates = jnp.concatenate([small, jnp.zeros((120, 256), F32)], axis=0).astype(BF16)
     gain_mid = small[2:3] + small[3:4] + small[4:5]
+    x = (xr * (small[5:6] + small[6:7] + small[7:8])).astype(BF16)
     lane32 = lax.broadcasted_iota(jnp.int32, (32, 128), 1)
 
     def with_square(block, sq, at):
@@ -188,23 +254,24 @@
         return jnp.where(lane32 == at, hi, jnp.where(lane32 == at + 1, sq - hi, block))
 
     gates = with_square(contract_last(x, wgates), square_in, 2)
-    arrive(2, w1g)
+    collected(2, w1g)
     q_part = jnp.dot(x, w1g[...].reshape(256, 256), preferred_element_type=F32)
     for j in range(8):
         mz1[j, :, 0:256] = q_part[4 * j : 4 * j + 4].astype(BF16)
         mz1[j, :, 256:384] = gates[4 * j : 4 * j + 4].astype(BF16)
-    rz1[z] = mz1[z]
-    send(6, lambda i: mz1.at[lax.bitwise_xor(z, i)], rz1.at[z], zs)
+    rz1[y] = mz1[y]
+    send(6, lambda i: mz1.at[lax.bitwise_xor(y, i)], rz1, y, ys)
     l_wu.wait()
-    send(7, lambda i: wug.at[y], wug.at[y], ys)
-    arrive(3, w2g)
+    spread(7, wug)
+    collected(3, w2g)
     kv_part = jnp.dot(x, w2g[...].reshape(256, 512), preferred_element_type=F32)
     for j in range(8):
         mz2[j] = kv_part[4 * j : 4 * j + 4].astype(BF16)
-    rz2[z] = mz2[z]
-    send(8, lambda i: mz2.at[lax.bitwise_xor(z, i)], rz2.at[z], zs)
+    rz2[y] = mz2[y]
+    send(8, lambda i: mz2.at[lax.bitwise_xor(y, i)], rz2, y, ys)
     l_wd.wait()
-    send(9, lambda i: wdg.at[y], wdg.at[y], ys)
+    relay(5, wmg)
+    spread(9, wdg)
 
     arrive(6, rz1)
     first = rz1[0].astype(F32)
@@ -246,34 +313,44 @@
     num = numerator[0:4] + (own_scale[0:4] * own_score) * second[:, 256:512]
     mixed = num * lax.rsqrt(jnp.mean(num * num, axis=1, keepdims=True) + EPS) * gh[...]
     mc[...] = mixed.astype(BF16)
-    rc[z] = mixed.astype(BF16)
-    send(10, lambda i: mc, rc.at[z], zs)
-
-    arrive(5, wmg)
+    rc[y] = mixed.astype(BF16)
+    send(10, lambda i: mc, rc, y, ys)
+    relay(7, wug)
+
+    collected(5, wmg)
     arrive(10, rc)
     for j in range(8):
         m32[4 * j : 4 * j + 4, :] = rc[j].astype(F32)
     att = contract_last(m32[...].astype(BF16), wmg[...].reshape(256, 256)).astype(BF16)
     md[...] = att
     rd[t] = att
-    send(11, lambda i: md, rd.at[t], ts)
+    send(11, lambda i: md, rd, t, ts)
+    relay(9, wdg)
     arrive(11, rd)
     attended = rd[0].astype(F32)
     for j in range(1, 8):
         attended += rd[j].astype(F32)
     restored = (xraw[...] + attended).astype(BF16).astype(F32)
-    for j in range(8):
-        res[j] = restored[4 * j : 4 * j + 4]
+    sent = contract_last(restored.astype(BF16), at_lanes(32, 32 * t, 256).astype(BF16)).astype(BF16)
+    mp[...] = sent
+
+    @pl.when(far)
+    def _():
+        start_one(14, mp, rp, rows_to(lax.bitwise_xor(z, t)))
+
+    @pl.when(z == t)
+    def _():
+        rp[...] = mp[...]
 
     square_mid = jnp.sum(restored * restored, axis=1, keepdims=True)
     sq_block = with_square(jnp.zeros((32, 128), F32), square_mid, 0)
-    arrive(7, wug)
+    collected(7, wug)
     up = jnp.dot((restored * gain_mid).astype(BF16), wug[...].reshape(256, 1024), preferred_element_type=F32)
     for j in range(8):
         mf[j, :, 0:1024] = up[4 * j : 4 * j + 4].astype(BF16)
         mf[j, :, 1024:1152] = sq_block[4 * j : 4 * j + 4].astype(BF16)
-    rf[z] = mf[z]
-    send(12, lambda i: mf.at[lax.bitwise_xor(z, i)], rf.at[z], zs)
+    rf[y] = mf[y]
+    send(12, lambda i: mf.at[lax.bitwise_xor(y, i)], rf, y, ys)
     arrive(12, rf)
     whole = rf[0].astype(F32)
     for j in range(1, 8):
@@ -281,37 +358,36 @@
     factor_mid = lax.rsqrt((whole[:, 1024:1025] + whole[:, 1025:1026]) / D + EPS)
     hid = jnp.square(jnp.maximum(whole[:, 0:1024] * factor_mid, 0.0)).astype(BF16)
     mg[...] = hid
-    rg[z] = hid
-    send(13, lambda i: mg, rg.at[z], zs)
-
-    arrive(9, wdg)
+    rg[y] = hid
+    send(13, lambda i: mg, rg, y, ys)
+
+    collected(9, wdg)
     arrive(13, rg)
     for j in range(8):
         h32[4 * j : 4 * j + 4, :] = rg[j].astype(F32)
     down = contract_last(h32[...].astype(BF16), wdg[...].reshape(256, 1024))
     for j in range(8):
-        mh[j] = down[4 * j : 4 * j + 4].astype(BF16)
-    rh[t] = mh[t]
-    send(14, lambda i: mh.at[lax.bitwise_xor(t, i)], rh.at[t], ts)
-    arrive(14, rh)
-    last = res[t]
+        mh[j] = down[:, 32 * j : 32 * j + 32].astype(BF16)
+    send_cross(15, lambda i: mh.at[lax.bitwise_xor(z, i)], rh, t, rows_of)
+
+    @pl.when(far)
+    def _():
+        pltpu.make_async_copy(rp, rp, rsem.at[14]).wait()
+
+    cross_done(rsem.at[15], rh)
     summed = rh[0].astype(F32)
     for j in range(1, 8):
         summed += rh[j].astype(F32)
-    done = (last + summed).astype(BF16)
-    mi[...] = done
-    ri[y] = done
-    send(15, lambda i: mi, ri.at[y], ys)
-    arrive(15, ri)
-    for j in range(8):
-        m32[4 * j : 4 * j + 4, :] = ri[j].astype(F32)
-    out_ref[...] = contract_last(m32[...].astype(BF16), place_b)
-
-    for n, buf in (
-        (0, ra), (1, a2), (2, w1g), (3, w2g), (4, rb), (5, wmg), (6, rz1), (7, wug), (8, rz2), (9, wdg), (10, rc), (11, rd),
-        (12, rf), (13, rg), (14, rh), (15, ri),
-    ):
+    out_ref[...] = rp[...].astype(F32) + summed
+
+    for n, buf in pending:
         left(n, buf)
+    cross_done(ssem.at[0], ra)
+    cross_done(ssem.at[15], rh)
+
+    @pl.when(far)
+    def _():
+        pltpu.make_async_copy(mp, mp, ssem.at[14]).wait()
 
 
 def body(
@@ -335,14 +411,13 @@
             vm((4, 1, 128), F32), vm((4, 1, 128), F32), vm((1, 4), jnp.int32), vm((1, 256), F32), vm((1, 32), F32),
             vm((8, 32, 256), BF16), vm((8, 32, 512), BF16), vm((8, 32, 256), BF16), vm((8, 32, 1024), BF16),
             vm((8, 32, 1024), BF16),
-            vm((8, 8, 256), BF16), vm((8, 8, 256), BF16), vm((8, 8, 256), BF16), vm((8, 256), BF16), vm((8, 8, 256), BF16),
-            vm((32, 256), F32), vm((32, 256), F32), vm((8, 4, 384), BF16), vm((8, 4, 384), BF16), vm((8, 4, 512), BF16),
+            vm((16, 128), BF16), vm((8, 16, 128), BF16), vm((8, 8, 128), BF16), vm((32, 256), F32), vm((8, 4, 384), BF16), vm((8, 4, 384), BF16), vm((8, 4, 512), BF16),
             vm((8, 4, 512), BF16), vm((4, 256, 256), BF16), vm((4, 256, 256), BF16), vm((3, 8, 128), F32), vm((16, 256), F32),
             vm((16, 128), F32), vm((4, 256), BF16), vm((8, 4, 256), BF16), vm((32, 256), F32), vm((32, 256), BF16),
-            vm((8, 32, 256), BF16), vm((8, 4, 256), F32), vm((8, 4, 1152), BF16), vm((8, 4, 1152), BF16), vm((4, 1024), BF16),
-            vm((8, 4, 1024), BF16), vm((32, 1024), F32), vm((8, 4, 256), BF16), vm((8, 4, 256), BF16), vm((4, 256), BF16),
-            vm((8, 4, 256), BF16),
-            pltpu.SemaphoreType.DMA((21,)), pltpu.SemaphoreType.DMA((16,)), pltpu.SemaphoreType.DMA((16,)),
+            vm((8, 32, 256), BF16), vm((8, 4, 1152), BF16), vm((8, 4, 1152), BF16), vm((4, 1024), BF16),
+            vm((8, 4, 1024), BF16), vm((32, 1024), F32), vm((8, 32, 32), BF16), vm((8, 32, 32), BF16), vm((32, 32), BF16),
+            vm((32, 32), BF16),
+            pltpu.SemaphoreType.DMA((21,)), pltpu.SemaphoreType.DMA((16,)), pltpu.SemaphoreType.DMA((48,)),
         ],
         compiler_params=pltpu.CompilerParams(collective_id=0, has_side_effects=True),
     )(*args)

time: 68.6 us -> 60.9 us (0.89)
  the two profiles are of different devices: /device:TPU:1 before, /device:TPU:4 now
where the time goes in v2:
time: 60.9 us; the launch traced here: 60.6 us
  Pallas kernels  58 us (95%)
  other arithmetic  1.32 us (2%)
  between operations  1.3 us (2%)
    pallas_call x1, Pallas kernels, body(): pl.pallas_call(kernel, out_shape=jax.ShapeDtypeStruct((32, 32), F32), in_...  58 us
    convert_element_type x1, other arithmetic, body(): return out.astype(BF16)  1.32 us

profile of v2, /device:TPU:4, one launch (start us, length us, event | category | flops | bytes accessed | tf_op | source)
XLA Modules:
  0.0 60.6 jit_solution(13533363670138666473)
XLA Ops:
  1.3 58.0 %shard_map.199 = f32[32,32]{1,0:T(8,128)} custom-call(bf16[32,32]{1,0:T(8,128)(2,1)} %tok_h.1, f32[1,32]{1,0:T(1,128)} %bitcast.16, bf16[32,256]{1,0:T(8,128)(2,1)} %wq_h.1, bf16[32,256]{1,0:T(8,128)(2,1)} %wk_h.1, bf16[32,256]{1,0:T(8,128)(2,1)} %wv_h.1, bf16[1,32]{1,0:T(2,128)(2,1)} %bitcast.17, bf16[1,32]{1,0:T(2,128)(2,1)} %bitcast.18, ...), custom_call_target="tpu_custom_call" | custom-call | tf_op jit(solution)/shard_map/pallas_call | solution.py:403
  59.3 1.3 %convert_element_type.3 = bf16[32,32]{1,0:T(8,128)(2,1)} convert(f32[32,32]{1,0:T(8,128)} %shard_map.199) | non-fusion elementwise | flops 1024 | bytes 6144 | tf_op jit(solution)/shard_map/convert_element_type | solution.py:424

commit v3 on v2

--- a/solution.py
+++ b/solution.py
@@ -10,6 +10,8 @@
 D = 2048
 EPS = 1e-06
 SCALE = 256 ** (-0.5)
+T_FAR_FIRST = (4, 5, 6, 7, 2, 3, 1)
+RING_FAR_FIRST = (4, 5, 3, 7, 6, 2, 1)
 
 
 def at_lanes(rows, offset, width):
@@ -34,8 +36,8 @@
     tok_h, gmix_h, wq_h, wk_h, wv_h, wi_h, wf_h, bi_h, bf_h, st_h, smax_h, k_h, v_h, ig_h, fg_h, len_h, gh_h, wm_h, gm_h,
     wu_h, wd_h, out_ref,
     tok, gmix, wi, wf, bi, bfg, st, smax, kb, vb, igb, fgb, lens, gh, gm,
-    w1g, w2g, wmg, wug, wdg,
-    ma, ra, a2, xraw, mz1, rz1, mz2, rz2, slo, shi, rows8, q16, w16, mc, rc, m32, md, rd, mf, rf, mg, rg, h32,
+    w1g, w2g, wmg, wug, wdo, wdg,
+    ma, ra, a2, xraw, mz1, rz1, mz2, rz2, slo, shi, rows8, q16, w16, mc, rc, m32, md, rd, mf, rf,
     mh, rh, mp, rp,
     lsem, ssem, rsem,
 ):
@@ -56,14 +58,18 @@
     def greet(who):
         pl.semaphore_signal(barrier, inc=1, device_id=who, device_id_type=MESH)
 
-    for who in (rows_to, rows_of, ys, zs, ts):
-        for i in range(1, 8):
-            greet(who(i))
-
     @pl.when(far)
     def _():
         greet(rows_to(0))
         greet(rows_of(0))
+
+    for i in T_FAR_FIRST:
+        greet(rows_to(i))
+    for who in (rows_of, zs, ys):
+        for i in RING_FAR_FIRST:
+            greet(who(i))
+    for i in T_FAR_FIRST:
+        greet(ts(i))
 
     loads = []
 
@@ -83,7 +89,9 @@
     l_wv = load(wv_h, w2g.at[z, :, pl.ds(256, 256)])
     l_wm = load(wm_h, wmg.at[z])
     l_wu = load(wu_h, wug.at[z])
-    l_wd = load(wd_h, wdg.at[z])
+    own_units = pl.ds(pl.multiple_of(128 * y, 128), 128)
+    l_wd = load(wd_h, wdo)
+    l_wdy = load(wd_h.at[:, own_units], wdg.at[z, y])
     cell = [
         load(a, b)
         for a, b in (
@@ -96,7 +104,7 @@
 
     def send(n, src, buf, slot, who):
         dst = buf.at[slot]
-        for i in range(1, 8):
+        for i in T_FAR_FIRST if who is ts else RING_FAR_FIRST:
             c = pltpu.make_async_remote_copy(
                 src_ref=src(i), dst_ref=dst, send_sem=ssem.at[n], recv_sem=rsem.at[n], device_id=who(i), device_id_type=MESH
             )
@@ -118,7 +126,7 @@
         ).start()
 
     def send_cross(n, src, buf, slot, who):
-        for i in range(1, 8):
+        for i in T_FAR_FIRST if who is rows_to else RING_FAR_FIRST:
             start_one(n, src(i), buf.at[slot], who(i))
 
         @pl.when(far)
@@ -137,26 +145,27 @@
             src_ref=chunk, dst_ref=chunk, send_sem=ssem.at[n], recv_sem=rsem.at[sem], device_id=who, device_id_type=MESH
         ).start()
 
-    def spread(n, buf):
-        for k in (2, -2, 1, -1):
-            relay_copy(n, buf.at[z], on_z(k), n if abs(k) == 2 else 16 + n)
-        pending.append((n, buf))
+    def spread(n, buf, ks=(2, -2, 1, -1)):
+        for k in ks:
+            relay_copy(n, buf.at[z], on_z(k), n if abs(k) == 2 else 24 + n)
+        if n not in arrived:
+            pending.append((n, buf))
         arrived.add(n)
 
     def relay(n, buf):
         part = buf.at[pl.ds(0, 2)]
         pltpu.make_async_copy(part, part, rsem.at[n]).wait()
         half = buf.shape[2] // 2
-        relay_copy(n, buf.at[zn(-2)], on_z(1), 32 + n)
-        relay_copy(n, buf.at[zn(2)], on_z(-1), 32 + n)
-        relay_copy(n, buf.at[zn(-2), :, pl.ds(0, half)], on_z(2), 32 + n)
-        relay_copy(n, buf.at[zn(2), :, pl.ds(half, half)], on_z(-2), 32 + n)
+        relay_copy(n, buf.at[zn(-2)], on_z(1), 48 + n)
+        relay_copy(n, buf.at[zn(2)], on_z(-1), 48 + n)
+        relay_copy(n, buf.at[zn(-2), :, pl.ds(0, half)], on_z(2), 48 + n)
+        relay_copy(n, buf.at[zn(2), :, pl.ds(half, half)], on_z(-2), 48 + n)
 
     def collected(n, buf):
         part = buf.at[pl.ds(0, 2)]
-        pltpu.make_async_copy(part, part, rsem.at[16 + n]).wait()
+        pltpu.make_async_copy(part, part, rsem.at[24 + n]).wait()
         part = buf.at[pl.ds(0, 3)]
-        pltpu.make_async_copy(part, part, rsem.at[32 + n]).wait()
+        pltpu.make_async_copy(part, part, rsem.at[48 + n]).wait()
 
     def cross_done(sem, buf):
         @pl.when(far)
@@ -165,7 +174,7 @@
 
         @pl.when(z == t)
         def _():
-            part = buf.at[pl.ds(0, 7)]
+            part = buf.at[pl.ds(0, buf.shape[0] - 1)]
             pltpu.make_async_copy(part, part, sem).wait()
 
     l_tok.wait()
@@ -194,10 +203,18 @@
     a2[z] = jnp.dot(eight.astype(BF16), place, preferred_element_type=F32).astype(BF16)
     send(1, lambda i: a2.at[z], a2, z, zs)
     l_w1.wait()
-    spread(2, w1g)
+    spread(2, w1g, (2, -2))
     l_wk.wait()
     l_wv.wait()
-    spread(3, w2g)
+    spread(3, w2g, (2, -2))
+    spread(2, w1g, (1, -1))
+    spread(3, w2g, (1, -1))
+    l_wd.wait()
+
+    def units(i):
+        return wdo.at[:, pl.ds(pl.multiple_of(128 * lax.bitwise_xor(y, i), 128), 128)]
+
+    send(16, units, wdg.at[z], y, ys)
 
     for c in cell:
         c.wait()
@@ -269,8 +286,9 @@
         mz2[j] = kv_part[4 * j : 4 * j + 4].astype(BF16)
     rz2[y] = mz2[y]
     send(8, lambda i: mz2.at[lax.bitwise_xor(y, i)], rz2, y, ys)
-    l_wd.wait()
     relay(5, wmg)
+    l_wdy.wait()
+    arrive(16, wdg.at[z])
     spread(9, wdg)
 
     arrive(6, rz1)
@@ -343,32 +361,54 @@
         rp[...] = mp[...]
 
     square_mid = jnp.sum(restored * restored, axis=1, keepdims=True)
-    sq_block = with_square(jnp.zeros((32, 128), F32), square_mid, 0)
+    tile = lax.broadcasted_iota(jnp.int32, (8, 128), 1)
+    high = square_mid.astype(BF16).astype(F32)
+    sq_rows = jnp.zeros((8, 128), F32)
+    for g in range(4):
+        sq_rows = jnp.where(tile == g, high[8 * g : 8 * g + 8], sq_rows)
+        sq_rows = jnp.where(tile == 4 + g, (square_mid - high)[8 * g : 8 * g + 8], sq_rows)
+    sq_rows = jnp.concatenate([sq_rows, jnp.zeros((8, 128), F32)], axis=0).astype(BF16)
     collected(7, wug)
     up = jnp.dot((restored * gain_mid).astype(BF16), wug[...].reshape(256, 1024), preferred_element_type=F32)
     for j in range(8):
-        mf[j, :, 0:1024] = up[4 * j : 4 * j + 4].astype(BF16)
-        mf[j, :, 1024:1152] = sq_block[4 * j : 4 * j + 4].astype(BF16)
+        mf[j, 0:32, :] = up[:, 128 * j : 128 * j + 128].astype(BF16)
+        mf[j, 32:48, :] = sq_rows
     rf[y] = mf[y]
     send(12, lambda i: mf.at[lax.bitwise_xor(y, i)], rf, y, ys)
     arrive(12, rf)
     whole = rf[0].astype(F32)
     for j in range(1, 8):
         whole += rf[j].astype(F32)
-    factor_mid = lax.rsqrt((whole[:, 1024:1025] + whole[:, 1025:1026]) / D + EPS)
-    hid = jnp.square(jnp.maximum(whole[:, 0:1024] * factor_mid, 0.0)).astype(BF16)
-    mg[...] = hid
-    rg[y] = hid
-    send(13, lambda i: mg, rg, y, ys)
-
+    squares = jnp.concatenate(
+        [whole[32:40, g : g + 1] + whole[32:40, 4 + g : 5 + g] for g in range(4)], axis=0
+    )
+    factor_mid = lax.rsqrt(squares / D + EPS)
+    hid = jnp.square(jnp.maximum(whole[0:32] * factor_mid, 0.0)).astype(BF16)
+
+    group = lax.shift_right_logical(tile, 5)
     collected(9, wdg)
-    arrive(13, rg)
-    for j in range(8):
-        h32[4 * j : 4 * j + 4, :] = rg[j].astype(F32)
-    down = contract_last(h32[...].astype(BF16), wdg[...].reshape(256, 1024))
-    for j in range(8):
-        mh[j] = down[:, 32 * j : 32 * j + 32].astype(BF16)
-    send_cross(15, lambda i: mh.at[lax.bitwise_xor(z, i)], rh, t, rows_of)
+    for jj in (*RING_FAR_FIRST, 0):
+        zz = lax.bitwise_xor(z, jj)
+        down = contract_last(hid, wdg[zz].reshape(256, 128))
+        for h in range(2):
+            part = down[:, 128 * h : 128 * h + 128]
+            turned = [part] + [pltpu.roll(part, 32 * k, 1) for k in range(1, 4)]
+            for d in range(4):
+                packed = jnp.zeros((8, 128), F32)
+                for g in range(4):
+                    packed = jnp.where(group == g, turned[(g - d) % 4][8 * g : 8 * g + 8], packed)
+                mh[8 * jj + 4 * h + d] = packed.astype(BF16)
+        for i in (*RING_FAR_FIRST, 0) if jj else RING_FAR_FIRST:
+            yy = lax.bitwise_xor(y, i)
+            start_one(15, mh.at[8 * jj + yy], rh.at[8 * t + y], (8 * zz + yy, z))
+
+    @pl.when(far)
+    def _():
+        start_one(15, mh.at[y], rh.at[8 * t + y], (kv, z))
+
+    @pl.when(z == t)
+    def _():
+        rh[8 * t + y] = mh[y]
 
     @pl.when(far)
     def _():
@@ -376,9 +416,11 @@
 
     cross_done(rsem.at[15], rh)
     summed = rh[0].astype(F32)
-    for j in range(1, 8):
+    for j in range(1, 64):
         summed += rh[j].astype(F32)
-    out_ref[...] = rp[...].astype(F32) + summed
+    for g in range(4):
+        rows = slice(8 * g, 8 * g + 8)
+        out_ref[rows, :] = rp[rows, :].astype(F32) + summed[:, 32 * g : 32 * g + 32]
 
     for n, buf in pending:
         left(n, buf)
@@ -402,7 +444,7 @@
     vm = pltpu.VMEM
     out = pl.pallas_call(
         kernel,
-        out_shape=jax.ShapeDtypeStruct((32, 32), F32),
+        out_shape=pltpu.VMEM((32, 32), F32),
         in_specs=[pl.BlockSpec(memory_space=pl.ANY)] * 21,
         out_specs=pl.BlockSpec(memory_space=pltpu.VMEM),
         scratch_shapes=[
@@ -410,14 +452,14 @@
             vm((4, 1, 256, 256), F32), vm((1, 4), F32), vm((4, 1, 128, 256), BF16), vm((4, 1, 128, 256), BF16),
             vm((4, 1, 128), F32), vm((4, 1, 128), F32), vm((1, 4), jnp.int32), vm((1, 256), F32), vm((1, 32), F32),
             vm((8, 32, 256), BF16), vm((8, 32, 512), BF16), vm((8, 32, 256), BF16), vm((8, 32, 1024), BF16),
-            vm((8, 32, 1024), BF16),
+            vm((32, 1024), BF16), vm((8, 8, 32, 128), BF16),
             vm((16, 128), BF16), vm((8, 16, 128), BF16), vm((8, 8, 128), BF16), vm((32, 256), F32), vm((8, 4, 384), BF16), vm((8, 4, 384), BF16), vm((8, 4, 512), BF16),
             vm((8, 4, 512), BF16), vm((4, 256, 256), BF16), vm((4, 256, 256), BF16), vm((3, 8, 128), F32), vm((16, 256), F32),
             vm((16, 128), F32), vm((4, 256), BF16), vm((8, 4, 256), BF16), vm((32, 256), F32), vm((32, 256), BF16),
-            vm((8, 32, 256), BF16), vm((8, 4, 1152), BF16), vm((8, 4, 1152), BF16), vm((4, 1024), BF16),
-            vm((8, 4, 1024), BF16), vm((32, 1024), F32), vm((8, 32, 32), BF16), vm((8, 32, 32), BF16), vm((32, 32), BF16),
+            vm((8, 32, 256), BF16), vm((8, 48, 128), BF16), vm((8, 48, 128), BF16),
+            vm((64, 8, 128), BF16), vm((64, 8, 128), BF16), vm((32, 32), BF16),
             vm((32, 32), BF16),
-            pltpu.SemaphoreType.DMA((21,)), pltpu.SemaphoreType.DMA((16,)), pltpu.SemaphoreType.DMA((48,)),
+            pltpu.SemaphoreType.DMA((22,)), pltpu.SemaphoreType.DMA((24,)), pltpu.SemaphoreType.DMA((72,)),
         ],
         compiler_params=pltpu.CompilerParams(collective_id=0, has_side_effects=True),
     )(*args)

time: 60.9 us -> 56.8 us (0.933)
  the two profiles are of different devices: /device:TPU:4 before, /device:TPU:1 now
where the time goes in v3:
time: 56.8 us; the launch traced here: 56.6 us
  Pallas kernels  54.7 us (96%)
  between operations  1.3 us (2%)
  other arithmetic  0.6 us (1%)
    pallas_call x1, Pallas kernels, body(): pl.pallas_call(kernel, out_shape=pltpu.VMEM((32, 32), F32), in_specs=[pl....  54.7 us

profile of v3, /device:TPU:1, one launch (start us, length us, event | category | flops | bytes accessed | tf_op | source)
XLA Modules:
  0.0 56.6 jit_solution(3191059690385449416)
XLA Ops:
  1.3 54.7 %shard_map.199 = f32[32,32]{1,0:T(8,128)S(1)} custom-call(bf16[32,32]{1,0:T(8,128)(2,1)} %tok_h.1, f32[1,32]{1,0:T(1,128)} %bitcast.16, bf16[32,256]{1,0:T(8,128)(2,1)} %wq_h.1, bf16[32,256]{1,0:T(8,128)(2,1)} %wk_h.1, bf16[32,256]{1,0:T(8,128)(2,1)} %wv_h.1, bf16[1,32]{1,0:T(2,128)(2,1)} %bitcast.17, bf16[1,32]{1,0:T(2,128)(2,1)} %bitcast.18, ...), custom_call_target="tpu_custom_call" | custom-call | tf_op jit(solution)/shard_map/pallas_call | solution.py:445
  56.0 0.6 %convert_element_type.3 = bf16[32,32]{1,0:T(8,128)(2,1)} convert(f32[32,32]{1,0:T(8,128)S(1)} %shard_map.199) | non-fusion elementwise | flops 1024 | bytes 6144 | tf_op jit(solution)/shard_map/convert_element_type | solution.py:466

commit v4 on v3

--- a/solution.py
+++ b/solution.py
@@ -68,8 +68,6 @@
     for who in (rows_of, zs, ys):
         for i in RING_FAR_FIRST:
             greet(who(i))
-    for i in T_FAR_FIRST:
-        greet(ts(i))
 
     loads = []
 
@@ -156,10 +154,10 @@
         part = buf.at[pl.ds(0, 2)]
         pltpu.make_async_copy(part, part, rsem.at[n]).wait()
         half = buf.shape[2] // 2
+        relay_copy(n, buf.at[zn(-2), :, pl.ds(0, half)], on_z(2), 48 + n)
+        relay_copy(n, buf.at[zn(2), :, pl.ds(half, half)], on_z(-2), 48 + n)
         relay_copy(n, buf.at[zn(-2)], on_z(1), 48 + n)
         relay_copy(n, buf.at[zn(2)], on_z(-1), 48 + n)
-        relay_copy(n, buf.at[zn(-2), :, pl.ds(0, half)], on_z(2), 48 + n)
-        relay_copy(n, buf.at[zn(2), :, pl.ds(half, half)], on_z(-2), 48 + n)
 
     def collected(n, buf):
         part = buf.at[pl.ds(0, 2)]
@@ -182,7 +180,7 @@
         tok[...], at_lanes(32, 32 * lax.bitwise_and(z, 1), 128).astype(BF16), preferred_element_type=F32
     )
     ma[...] = (placed[0:16] + pltpu.roll(placed[16:32], 64, 1)).astype(BF16)
-    pl.semaphore_wait(barrier, 37 - 2 * (z == t).astype(jnp.int32))
+    pl.semaphore_wait(barrier, 30 - 2 * (z == t).astype(jnp.int32))
     send_cross(0, lambda i: ma, ra, z, rows_to)
 
     l_wi.wait()
@@ -201,13 +199,13 @@
     for r, v in enumerate((wi[...].astype(F32), wf[...].astype(F32), *parts(gm[...]), *parts(gmix[...]))):
         eight = jnp.where(row8 == r, jnp.broadcast_to(v, (8, 32)), eight)
     a2[z] = jnp.dot(eight.astype(BF16), place, preferred_element_type=F32).astype(BF16)
-    send(1, lambda i: a2.at[z], a2, z, zs)
     l_w1.wait()
     spread(2, w1g, (2, -2))
     l_wk.wait()
     l_wv.wait()
     spread(3, w2g, (2, -2))
     spread(2, w1g, (1, -1))
+    send(1, lambda i: a2.at[z], a2, z, zs)
     spread(3, w2g, (1, -1))
     l_wd.wait()
 
@@ -218,10 +216,6 @@
 
     for c in cell:
         c.wait()
-    for s in range(4):
-        hi = st[s, 0].astype(BF16)
-        shi[s] = hi
-        slo[s] = (st[s, 0] - hi.astype(F32)).astype(BF16)
     rows8[...] = jnp.zeros(rows8.shape, F32)
     for s in range(4):
         rows8[0, s : s + 1, :] = igb[s]
@@ -291,6 +285,10 @@
     arrive(16, wdg.at[z])
     spread(9, wdg)
 
+    for s in range(4):
+        hi = st[s, 0].astype(BF16)
+        shi[s] = hi
+        slo[s] = (st[s, 0] - hi.astype(F32)).astype(BF16)
     arrive(6, rz1)
     first = rz1[0].astype(F32)
     for j in range(1, 8):

time: 56.8 us -> 56.3 us (level)
  no operation moved by 1% of the time
where the time goes in v4:
time: 56.3 us; the launch traced here: 56.1 us
  Pallas kernels  54.2 us (96%)
  between operations  1.3 us (2%)
  other arithmetic  0.6 us (1%)
    pallas_call x1, Pallas kernels, body(): pl.pallas_call(kernel, out_shape=pltpu.VMEM((32, 32), F32), in_specs=[pl....  54.2 us

profile of v4, /device:TPU:1, one launch (start us, length us, event | category | flops | bytes accessed | tf_op | source)
XLA Modules:
  0.0 56.1 jit_solution(3083688501743306228)
XLA Ops:
  1.3 54.2 %shard_map.199 = f32[32,32]{1,0:T(8,128)S(1)} custom-call(bf16[32,32]{1,0:T(8,128)(2,1)} %tok_h.1, f32[1,32]{1,0:T(1,128)} %bitcast.16, bf16[32,256]{1,0:T(8,128)(2,1)} %wq_h.1, bf16[32,256]{1,0:T(8,128)(2,1)} %wk_h.1, bf16[32,256]{1,0:T(8,128)(2,1)} %wv_h.1, bf16[1,32]{1,0:T(2,128)(2,1)} %bitcast.17, bf16[1,32]{1,0:T(2,128)(2,1)} %bitcast.18, ...), custom_call_target="tpu_custom_call" | custom-call | tf_op jit(solution)/shard_map/pallas_call | solution.py:443
  55.5 0.6 %convert_element_type.3 = bf16[32,32]{1,0:T(8,128)(2,1)} convert(f32[32,32]{1,0:T(8,128)S(1)} %shard_map.199) | non-fusion elementwise | flops 1024 | bytes 6144 | tf_op jit(solution)/shard_map/convert_element_type | solution.py:464

commit v5 on v4

--- a/solution.py
+++ b/solution.py
@@ -270,8 +270,8 @@
     for j in range(8):
         mz1[j, :, 0:256] = q_part[4 * j : 4 * j + 4].astype(BF16)
         mz1[j, :, 256:384] = gates[4 * j : 4 * j + 4].astype(BF16)
+    send(6, lambda i: mz1.at[lax.bitwise_xor(y, i)], rz1, y, ys)
     rz1[y] = mz1[y]
-    send(6, lambda i: mz1.at[lax.bitwise_xor(y, i)], rz1, y, ys)
     l_wu.wait()
     spread(7, wug)
     collected(3, w2g)
@@ -329,8 +329,8 @@
     num = numerator[0:4] + (own_scale[0:4] * own_score) * second[:, 256:512]
     mixed = num * lax.rsqrt(jnp.mean(num * num, axis=1, keepdims=True) + EPS) * gh[...]
     mc[...] = mixed.astype(BF16)
+    send(10, lambda i: mc, rc, y, ys)
     rc[y] = mixed.astype(BF16)
-    send(10, lambda i: mc, rc, y, ys)
     relay(7, wug)
 
     collected(5, wmg)
@@ -339,24 +339,14 @@
         m32[4 * j : 4 * j + 4, :] = rc[j].astype(F32)
     att = contract_last(m32[...].astype(BF16), wmg[...].reshape(256, 256)).astype(BF16)
     md[...] = att
+    send(11, lambda i: md, rd, t, ts)
     rd[t] = att
-    send(11, lambda i: md, rd, t, ts)
     relay(9, wdg)
     arrive(11, rd)
     attended = rd[0].astype(F32)
     for j in range(1, 8):
         attended += rd[j].astype(F32)
     restored = (xraw[...] + attended).astype(BF16).astype(F32)
-    sent = contract_last(restored.astype(BF16), at_lanes(32, 32 * t, 256).astype(BF16)).astype(BF16)
-    mp[...] = sent
-
-    @pl.when(far)
-    def _():
-        start_one(14, mp, rp, rows_to(lax.bitwise_xor(z, t)))
-
-    @pl.when(z == t)
-    def _():
-        rp[...] = mp[...]
 
     square_mid = jnp.sum(restored * restored, axis=1, keepdims=True)
     tile = lax.broadcasted_iota(jnp.int32, (8, 128), 1)
@@ -371,8 +361,18 @@
     for j in range(8):
         mf[j, 0:32, :] = up[:, 128 * j : 128 * j + 128].astype(BF16)
         mf[j, 32:48, :] = sq_rows
+    send(12, lambda i: mf.at[lax.bitwise_xor(y, i)], rf, y, ys)
     rf[y] = mf[y]
-    send(12, lambda i: mf.at[lax.bitwise_xor(y, i)], rf, y, ys)
+    sent = contract_last(restored.astype(BF16), at_lanes(32, 32 * t, 256).astype(BF16)).astype(BF16)
+    mp[...] = sent
+
+    @pl.when(far)
+    def _():
+        start_one(14, mp, rp, rows_to(lax.bitwise_xor(z, t)))
+
+    @pl.when(z == t)
+    def _():
+        rp[...] = mp[...]
     arrive(12, rf)
     whole = rf[0].astype(F32)
     for j in range(1, 8):

time: 56.3 us -> 56.2 us (level)
  no operation moved by 1% of the time
where the time goes in v5:
time: 56.2 us; the launch traced here: 56 us
  Pallas kernels  54.1 us (96%)
  between operations  1.3 us (2%)
  other arithmetic  0.6 us (1%)
    pallas_call x1, Pallas kernels, body(): pl.pallas_call(kernel, out_shape=pltpu.VMEM((32, 32), F32), in_specs=[pl....  54.1 us

profile of v5, /device:TPU:1, one launch (start us, length us, event | category | flops | bytes accessed | tf_op | source)
XLA Modules:
  0.0 56.0 jit_solution(16059969394900314757)
XLA Ops:
  1.3 54.1 %shard_map.199 = f32[32,32]{1,0:T(8,128)S(1)} custom-call(bf16[32,32]{1,0:T(8,128)(2,1)} %tok_h.1, f32[1,32]{1,0:T(1,128)} %bitcast.16, bf16[32,256]{1,0:T(8,128)(2,1)} %wq_h.1, bf16[32,256]{1,0:T(8,128)(2,1)} %wk_h.1, bf16[32,256]{1,0:T(8,128)(2,1)} %wv_h.1, bf16[1,32]{1,0:T(2,128)(2,1)} %bitcast.17, bf16[1,32]{1,0:T(2,128)(2,1)} %bitcast.18, ...), custom_call_target="tpu_custom_call" | custom-call | tf_op jit(solution)/shard_map/pallas_call | solution.py:443
  55.4 0.6 %convert_element_type.3 = bf16[32,32]{1,0:T(8,128)(2,1)} convert(f32[32,32]{1,0:T(8,128)S(1)} %shard_map.199) | non-fusion elementwise | flops 1024 | bytes 6144 | tf_op jit(solution)/shard_map/convert_element_type | solution.py:464
